TPU v7x, 128 devices: a whole 4x4x4 slice. The times are simulated.
128 devices in a mesh: rep: 2 (over z_hi), fs: 32 (over z_lo, y, x), tp: 2 (over core).
Axes of the slice: x: 4, y: 4, z: 4 (z_hi: 2, z_lo: 2; z = z_hi * 2 + z_lo), core: 2. Of those that a mesh axis runs over, the one named last changes fastest.
Arguments:
- stream_in: bfloat16 [64, 1024, 2048], P(('rep', 'fs'), None, 'tp'), may hold values from -48 to 48
- decay_shift: float32 [64, 1024], P(('rep', 'fs')), may hold values from -1.5 to 0, as said below
- mixer_gain: float32 [2048], replicated, may hold values from 0.1 to 1.9
- gate_weight: bfloat16 [2048, 1024], P('fs', 'tp'), may hold values from -0.125 to 0.125
- input_weight: bfloat16 [2048, 1024], P('fs', 'tp'), may hold values from -0.125 to 0.125
- filter_taps: float32 [4, 1024], P(None, 'tp'), may hold values from -3 to 3
- recur_gate: bfloat16 [4, 256, 256], P('tp'), may hold values from -0.375 to 0.375
- inlet_gate: bfloat16 [4, 256, 256], P('tp'), may hold values from -0.375 to 0.375
- decay_param: float32 [1024], P('tp'), may hold values from 1.5 to 12
- mixer_out: bfloat16 [1024, 2048], P('tp', 'fs'), may hold values from -0.1875 to 0.1875
- feedforward_gain: float32 [2048], replicated, may hold values from 0.1 to 1.9
- up_weight: bfloat16 [2048, 4096], P('fs', 'tp'), may hold values from -0.125 to 0.125
- down_weight: bfloat16 [4096, 2048], P('tp', 'fs'), may hold values from -0.09375 to 0.09375
- final_gain: float32 [2048], P('tp'), may hold values from 0.1 to 1.9
Outputs:
- layer_out: bfloat16 [64, 1024, 2048], P(('rep', 'fs'), None, 'tp')
Inputs may be any that keep to these rules, and one draw needn't show every extreme that they name: `decay_shift`: every entry is negative.
All inputs are finite; a program needn't handle non-finite values.
Results may differ from a plain program's by a relative error of at most 0.015.
Values may be sent and summed in bfloat16 or wider, within the bound.
No kernel may reach another device: no remote copies, remote signals or barrier semaphores. Data moves between devices by JAX's collectives and lax.ppermute only.
A program may use at most 128 MiB of HBM per device.

v0:
```python
import jax
import jax.numpy as jnp
from jax import lax
from jax.sharding import PartitionSpec as P

D = 2048
epsilon = 1e-06
rate_scale = 8.0


def rows_first(arrays, axis, dims):
    turned = [jnp.moveaxis(a, dim, 0) for a, dim in zip(arrays, dims)]
    widths = [t[0].size for t in turned]
    both = jnp.concatenate([t.reshape(-1, w) for t, w in zip(turned, widths)], axis=1)
    out = lax.all_gather(both, axis, axis=0, tiled=True)
    parts = jnp.split(out, [sum(widths[:k]) for k in range(1, len(widths))], axis=1)
    return tuple(
        (
            jnp.moveaxis(b.reshape(-1, *t.shape[1:]), 0, dim)
            for b, t, dim in zip(parts, turned, dims)
        )
    )


def side_by_side(arrays, axis, dim, along):
    ends, at = ([], 0)
    for a in arrays[:-1]:
        at += a.shape[along]
        ends.append(at)
    both = jnp.concatenate(arrays, axis=along)
    return tuple(jnp.split(lax.all_gather(both, axis, axis=dim, tiled=True), ends, axis=along))


def cut_along(x, dim, size):
    before, after = (x.shape[:dim], x.shape[dim + 1 :])
    return jnp.moveaxis(x.reshape(*before, size, -1, *after), dim, 0)


def summed_on_arrival(x, axis, dim):
    parts = cut_along(x, dim, lax.axis_size(axis))
    arrived = lax.all_to_all(parts, axis, split_axis=0, concat_axis=0, tiled=True)
    return arrived.astype(jnp.float32).sum(axis=0)


def from_everyone(x, axis):
    copies = jnp.broadcast_to(x, (lax.axis_size(axis), *x.shape))
    return lax.all_to_all(copies, axis, split_axis=0, concat_axis=0, tiled=True)


def over_copies(x, axis):
    return from_everyone(x, axis).sum(axis=0)


def norm_rows(values, row_gain):
    mean_sq = jnp.mean(values * values, axis=-1, keepdims=True)
    return values * lax.rsqrt(mean_sq + epsilon) * row_gain


def combine(earlier, later):
    return (earlier[0] * later[0], later[0] * earlier[1] + later[1])


def local(
    stream_in,
    decay_shift,
    mixer_gain,
    gate_weight,
    input_weight,
    filter_taps,
    recur_gate,
    inlet_gate,
    decay_param,
    mixer_out,
    feedforward_gain,
    up_weight,
    down_weight,
    final_gain,
):
    num_seq, length, half_width = stream_in.shape
    up_whole, complete_contraction = rows_first((up_weight, down_weight), "fs", (0, 1))
    whole = lax.all_gather(stream_in, "tp", axis=2, tiled=True)
    flat_rows = num_seq * length
    normed = norm_rows(whole.reshape(flat_rows, -1).astype(jnp.float32), mixer_gain).astype(
        jnp.bfloat16
    )
    channels = gate_weight.shape[1]
    fragments = side_by_side((gate_weight, input_weight), "fs", 0, 1)
    gate_logits = jnp.dot(normed, fragments[0], preferred_element_type=jnp.float32)
    input_pre = jnp.dot(normed, fragments[1], preferred_element_type=jnp.float32)
    gate_logits = gate_logits.astype(jnp.bfloat16)
    input_pre = input_pre.astype(jnp.bfloat16)
    branch = jax.nn.gelu(gate_logits.astype(jnp.float32), approximate=True)
    num_taps = filter_taps.shape[0]
    extended_front = jnp.pad(
        input_pre.astype(jnp.float32).reshape(num_seq, length, channels),
        ((0, 0), (num_taps - 1, 0), (0, 0)),
    )
    filtered = jnp.zeros((num_seq, length, channels), jnp.float32)
    for offset in range(num_taps):
        filtered = (
            filtered
            + extended_front[:, offset : offset + length] * filter_taps[offset][None, None, :]
        )
    filtered = filtered.astype(jnp.bfloat16).reshape(flat_rows, channels)
    num_blocks = recur_gate.shape[0]
    grouped = filtered.reshape(flat_rows, num_blocks, recur_gate.shape[1])
    recur = jax.nn.sigmoid(
        jnp.einsum("lni,nij->lnj", grouped, recur_gate, preferred_element_type=jnp.float32).reshape(
            flat_rows, channels
        )
    )
    inlet = jax.nn.sigmoid(
        jnp.einsum("lni,nij->lnj", grouped, inlet_gate, preferred_element_type=jnp.float32).reshape(
            flat_rows, channels
        )
    )
    logarithm_decay = (
        -rate_scale * recur * jax.nn.softplus(-decay_param)[None, :]
        + decay_shift.reshape(flat_rows)[:, None]
    )
    decay = jnp.exp(logarithm_decay).reshape(num_seq, length, channels)
    drive = (
        jnp.sqrt(-jnp.expm1(2.0 * logarithm_decay)) * inlet * filtered.astype(jnp.float32)
    ).reshape(num_seq, length, channels)
    states = lax.associative_scan(combine, (decay, drive), axis=1)[1]
    mixed = (states.reshape(flat_rows, channels) * branch).astype(jnp.bfloat16)
    mixer_terms = (
        jnp.dot(
            mixed,
            lax.all_gather(mixer_out, "fs", axis=1, tiled=True),
            preferred_element_type=jnp.float32,
        )
        .astype(jnp.bfloat16)
        .astype(jnp.float32)
    )
    mixer_sum = summed_on_arrival(mixer_terms.astype(jnp.bfloat16), "tp", 1)
    stream_mid = (stream_in.reshape(flat_rows, half_width).astype(jnp.float32) + mixer_sum).astype(
        jnp.bfloat16
    )
    stream_whole = lax.all_gather(stream_mid, "tp", axis=1, tiled=True)
    normed_mid = norm_rows(stream_whole.astype(jnp.float32), feedforward_gain).astype(jnp.bfloat16)
    up_proj = jnp.dot(normed_mid, up_whole, preferred_element_type=jnp.float32)
    activated = jnp.square(jax.nn.relu(up_proj)).astype(jnp.bfloat16)
    ffn_terms = (
        jnp.dot(activated, complete_contraction, preferred_element_type=jnp.float32)
        .astype(jnp.bfloat16)
        .astype(jnp.float32)
    )
    ffn_sum = summed_on_arrival(ffn_terms.astype(jnp.bfloat16), "tp", 1)
    total = stream_mid.astype(jnp.float32) + ffn_sum
    squares_sum = over_copies(jnp.sum(total * total, axis=1), "tp")
    layer_out = total * lax.rsqrt(squares_sum / D + epsilon)[:, None] * final_gain[None, :]
    return layer_out.astype(jnp.bfloat16).reshape(num_seq, length, half_width)


def solution(mesh):
    return jax.shard_map(
        local,
        mesh=mesh,
        in_specs=(
            P(("rep", "fs"), None, "tp"),
            P(("rep", "fs"), None),
            P(),
            P("fs", "tp"),
            P("fs", "tp"),
            P(None, "tp"),
            P("tp", None, None),
            P("tp", None, None),
            P("tp"),
            P("tp", "fs"),
            P(),
            P("fs", "tp"),
            P("tp", "fs"),
            P("tp"),
        ),
        out_specs=P(("rep", "fs"), None, "tp"),
        check_vma=False,
    )
```

profile of v0, /device:TPU:1, one launch (start us, length us, event | category | flops | bytes accessed | tf_op | source)
XLA Modules:
  0.0 648.5 jit_solution(12053179371689697069)
XLA Ops:
  11.2 17.8 %all-gather.6.cloned.1.call-done = bf16[1,1024,2048]{2,1,0:T(8,128)(2,1)} async-done(((bf16[1,1024,1024]{2,1,0:T(8,128)(2,1)}), bf16[1,1024,2048]{2,1,0:T(8,128)(2,1)}) %all-gather.6.cloned.1.call-update) | async-done | bytes 4194320 | tf_op jit(solution)/shard_map/all_gather | solution.py:81
  29.0 3.1 fusion.3
  32.1 135.9 %all-gather.8.cloned.1.call-done = bf16[2048,1024]{1,0:T(8,128)(2,1)} async-done(((bf16[64,1024]{1,0:T(8,128)(2,1)}), bf16[2048,1024]{1,0:T(8,128)(2,1)}) %all-gather.8.cloned.1.call-update) | async-done | bytes 4194320 | tf_op jit(solution)/shard_map/all_gather | solution.py:31
  168.0 5.2 fusion.39
  183.6 5.2 fusion.38
  188.8 3.5 slice.263
  192.2 3.5 slice.264
  195.7 6.3 slice.262
  202.0 6.3 slice.266
  208.2 3.7 fusion.83
  216.0 3.6 slice.268
  219.7 3.6 slice.272
  296.2 3.7 slice.267
  303.5 6.3 slice.261
  321.5 8.7 %pad.85 = f32[1,1024,512]{2,1,0:T(8,128)} pad(f32[1,512,512]{2,1,0:T(8,128)} %add.272, f32[]{:T(128)} %constant.10.clone.1), padding=0_0_0x1_0_1x0_0_0 | pad | bytes 3145732 | tf_op jit(solution)/shard_map/pad | solution.py:125
  332.1 4.7 pad.84
  336.8 11.0 %convolution_convert_fusion = bf16[1024,2048]{1,0:T(8,128)(2,1)} fusion(bf16[512,2048]{0,1:T(8,128)(2,1)} %all-gather.10.cloned.1.call-done, f32[1,1024,512]{2,1,0:T(8,128)} %pad.84, f32[1,1024,512]{2,1,0:T(8,128)S(1)} %copy-done.8, bf16[2048,1024]{1,0:T(8,128)(2,1)} %all-gather.8.cloned.1.call-done, ...), kind=kOutput, calls=%fused_computation.32 | convolution fusion | flops 4312268800 | bytes 16789504 | tf_op jit(solution)/shard_map/dot_general | solution.py:128
  350.5 27.4 %all_to_all.16 = bf16[2,1024,1024]{2,1,0:T(8,128)(2,1)S(1)} all-to-all(bf16[2,1024,1024]{2,1,0:T(8,128)(2,1)S(1)} %bitcast.68), channel_id=1, replica_groups=mesh['rep'=2,'fs'=32,'tp'=2] {'tp'}, dimensions={0} | all-to-all | bytes 8388608 | tf_op jit(solution)/shard_map/all_to_all | solution.py:41
  384.1 16.1 %all-gather.12.cloned.1.call-done = bf16[1024,2048]{1,0:T(8,128)(2,1)} async-done(((bf16[1024,1024]{1,0:T(8,128)(2,1)}), bf16[1024,2048]{1,0:T(8,128)(2,1)}) %all-gather.12.cloned.1.call-update) | async-done | bytes 4194320 | tf_op jit(solution)/shard_map/all_gather | solution.py:140
  403.3 189.5 %all-gather.14.cloned.1.call-done = bf16[2048,4096]{1,0:T(8,128)(2,1)} async-done(((bf16[64,4096]{1,0:T(8,128)(2,1)}), bf16[2048,4096]{1,0:T(8,128)(2,1)}) %all-gather.14.cloned.1.call-update) | async-done | bytes 16777232 | tf_op jit(solution)/shard_map/all_gather | solution.py:15
  592.9 25.7 %fusion.21 = bf16[1024,2048]{1,0:T(8,128)(2,1)} fusion(bf16[2048,4096]{1,0:T(8,128)(2,1)} %all-gather.14.cloned.1.call-done, bf16[1024,2048]{1,0:T(8,128)(2,1)} %all-gather.12.cloned.1.call-done, f32[2048]{0:T(1024)S(1)} %copy-done.33, f32[1024]{0:T(1024)S(1)} %add_rsqrt_fusion.1), kind=kOutput, calls=%fused_computation.31 | convolution fusion | flops 17196646400 | bytes 25178112 | tf_op jit(solution)/shard_map/dot_general | solution.py:145
  621.2 7.8 %all_to_all.17 = bf16[2,1024,1024]{2,1,0:T(8,128)(2,1)S(1)} all-to-all(bf16[2,1024,1024]{2,1,0:T(8,128)(2,1)S(1)} %bitcast.69), channel_id=1, replica_groups=mesh['rep'=2,'fs'=32,'tp'=2] {'tp'}, dimensions={0} | all-to-all | bytes 8388608 | tf_op jit(solution)/shard_map/all_to_all | solution.py:41
  632.6 3.7 all_to_all.18
  636.4 5.6 fusion.18
  (206 shorter events, 126.8 us)
Async XLA Ops:
  6.5 169.3 %copy-start = (bf16[2,256,256]{2,1,0:T(8,128)(2,1)S(1)}, bf16[2,256,256]{2,1,0:T(8,128)(2,1)}, u32[]{:S(2)}) copy-start(bf16[2,256,256]{2,1,0:T(8,128)(2,1)} %param.20) | copy-start | bytes 786436
  6.5 161.5 %copy-start.31 = (f32[2048]{0:T(1024)S(1)}, f32[2048]{0:T(1024)}, u32[]{:S(2)}) copy-start(f32[2048]{0:T(1024)} %param.16) | copy-start | bytes 24580
  6.5 22.5 %all-gather.6.cloned.1.call-start = ((), (), s32[]{:S(2)}) async-start(), calls=%async_computation.3 | async-start | bytes 6291456 | tf_op jit(solution)/shard_map/all_gather | solution.py:81
  7.3 160.7 %all-gather.8.cloned.1.call-start = ((), (), s32[]{:S(2)}) async-start(), calls=%async_computation.4 | async-start | bytes 4325376 | tf_op jit(solution)/shard_map/all_gather | solution.py:31
  8.9 327.9 %all-gather.10.cloned.1.call-start = ((), (), s32[]{:S(2)}) async-start(), calls=%async_computation.5 | async-start | bytes 2162688 | tf_op jit(solution)/shard_map/all_gather | solution.py:130
  9.6 390.6 %all-gather.12.cloned.1.call-start = ((), (), s32[]{:S(2)}) async-start(), calls=%async_computation.6 | async-start | bytes 6291456 | tf_op jit(solution)/shard_map/all_gather | solution.py:140
  32.1 141.1 %copy-start.28 = (f32[1024]{0:T(1024)}, f32[1024]{0:T(1024)S(1)}, u32[]{:S(2)}) copy-start(f32[1024]{0:T(1024)S(1)} %add_rsqrt_fusion.2) | copy-start | bytes 12292
  289.8 20.6 %copy-start.17 = (f32[1,2,512]{2,1,0:T(2,128)S(1)}, f32[1,2,512]{2,1,0:T(2,128)}, u32[]{:S(2)}) copy-start(f32[1,2,512]{2,1,0:T(2,128)} %slice.310) | copy-start | bytes 12292
  289.8 20.6 %copy-start.18 = (f32[1,2,512]{2,1,0:T(2,128)S(1)}, f32[1,2,512]{2,1,0:T(2,128)}, u32[]{:S(2)}) copy-start(f32[1,2,512]{2,1,0:T(2,128)} %slice.311) | copy-start | bytes 12292
  289.8 20.6 %copy-start.19 = (f32[1,2,512]{2,1,0:T(2,128)S(1)}, f32[1,2,512]{2,1,0:T(2,128)}, u32[]{:S(2)}) copy-start(f32[1,2,512]{2,1,0:T(2,128)} %slice.312) | copy-start | bytes 12292
  289.8 20.6 %copy-start.20 = (f32[1,2,512]{2,1,0:T(2,128)S(1)}, f32[1,2,512]{2,1,0:T(2,128)}, u32[]{:S(2)}) copy-start(f32[1,2,512]{2,1,0:T(2,128)} %slice.314) | copy-start | bytes 12292
  289.8 20.6 %copy-start.14 = (f32[1,4,512]{2,1,0:T(4,128)S(1)}, f32[1,4,512]{2,1,0:T(4,128)}, u32[]{:S(2)}) copy-start(f32[1,4,512]{2,1,0:T(4,128)} %get-tuple-element.24) | copy-start | bytes 24580
  289.8 21.4 %copy-start.15 = (f32[1,3,512]{2,1,0:T(4,128)S(1)}, f32[1,3,512]{2,1,0:T(4,128)}, u32[]{:S(2)}) copy-start(f32[1,3,512]{2,1,0:T(4,128)} %slice.303) | copy-start | bytes 18436
  289.8 21.4 %copy-start.16 = (f32[1,3,512]{2,1,0:T(4,128)S(1)}, f32[1,3,512]{2,1,0:T(4,128)}, u32[]{:S(2)}) copy-start(f32[1,3,512]{2,1,0:T(4,128)} %slice.320) | copy-start | bytes 18436
  289.8 21.4 %copy-start.25 = (f32[1,1,512]{2,1,0:T(1,128)S(1)}, f32[1,1,512]{2,1,0:T(1,128)}, u32[]{:S(2)}) copy-start(f32[1,1,512]{2,1,0:T(1,128)} %slice.342) | copy-start | bytes 6148
  289.8 21.5 %copy-start.13 = (f32[1,7,512]{2,1,0:T(8,128)S(1)}, f32[1,7,512]{2,1,0:T(8,128)}, u32[]{:S(2)}) copy-start(f32[1,7,512]{2,1,0:T(8,128)} %slice.322) | copy-start | bytes 43012
  289.9 21.5 %copy-start.24 = (f32[1,1,512]{2,1,0:T(1,128)S(1)}, f32[1,1,512]{2,1,0:T(1,128)}, u32[]{:S(2)}) copy-start(f32[1,1,512]{2,1,0:T(1,128)} %slice.341) | copy-start | bytes 6148
  289.9 21.6 %copy-start.11 = (f32[1,15,512]{2,1,0:T(8,128)S(1)}, f32[1,15,512]{2,1,0:T(8,128)}, u32[]{:S(2)}) copy-start(f32[1,15,512]{2,1,0:T(8,128)} %slice.291) | copy-start | bytes 92164
  289.9 21.6 %copy-start.12 = (f32[1,15,512]{2,1,0:T(8,128)S(1)}, f32[1,15,512]{2,1,0:T(8,128)}, u32[]{:S(2)}) copy-start(f32[1,15,512]{2,1,0:T(8,128)} %slice.324) | copy-start | bytes 92164
  289.9 21.6 %copy-start.23 = (f32[1,1,512]{2,1,0:T(1,128)S(1)}, f32[1,1,512]{2,1,0:T(1,128)}, u32[]{:S(2)}) copy-start(f32[1,1,512]{2,1,0:T(1,128)} %slice.340) | copy-start | bytes 6148
  321.5 10.4 %copy-start.21 = (f32[1,1,512]{2,1,0:T(1,128)S(1)}, f32[1,1,512]{2,1,0:T(1,128)}, u32[]{:S(2)}) copy-start(f32[1,1,512]{2,1,0:T(1,128)} %slice.335) | copy-start | bytes 6148
  330.2 6.6 %copy-start.32 = (f32[2048]{0:T(1024)S(1)}, f32[2048]{0:T(1024)}, u32[]{:S(2)}) copy-start(f32[2048]{0:T(1024)} %param.16) | copy-start | bytes 24580
  383.1 209.7 %copy-start.33 = (f32[2048]{0:T(1024)S(1)}, f32[2048]{0:T(1024)}, u32[]{:S(2)}) copy-start(f32[2048]{0:T(1024)} %param.24) | copy-start | bytes 24580
  383.1 209.7 %all-gather.14.cloned.1.call-start = ((), (), s32[]{:S(2)}) async-start(), calls=%async_computation.7 | async-start | bytes 17301504 | tf_op jit(solution)/shard_map/all_gather | solution.py:15
  (15 other events, 55.4 us)
Sparse Core Ops, SparseCore 0:
  9.0 19.9 all-gather.5
  30.7 137.2 all-gather.7
  169.6 151.5 all-gather.9
  383.3 16.9 all-gather.11
  401.7 191.0 all-gather.13
where the time goes:
time: 652 us; the launch traced here: 649 us
  waiting for transfers between devices  361 us (55%)
  local copies, waits for them, and re-layouts  137 us (21%)
  other arithmetic  52.2 us (8%)
  matrix products  45.9 us (7%)
  blocking collectives  38.9 us (6%)
  between operations  13.8 us (2%)
    all_gather x1, waiting for transfers between devices, rows_first(): out = lax.all_gather(both, axis, axis=0, tiled=True)  190 us
    all_gather x1, waiting for transfers between devices, side_by_side(): lax.all_gather(both, axis, axis=dim, tiled=True)  136 us
    slice x60, local copies, waits for them, and re-layouts, local(): states = lax.associative_scan(combine, (decay, drive), axis=1)[1]  106 us
    all_to_all x2, blocking collectives, summed_on_arrival(): lax.all_to_all(parts, axis, split_axis=0, concat_axis=0, tiled=True)  35.2 us
    dot_general x1, matrix products, local(): jnp.dot(activated, complete_contraction, preferred_element_type=jnp.float32)  25.7 us
    all_gather x1, waiting for transfers between devices, local(): whole = lax.all_gather(stream_in, 'tp', axis=2, tiled=True)  17.8 us
    all_gather x1, waiting for transfers between devices, local(): stream_whole = lax.all_gather(stream_mid, 'tp', axis=1, tiled=True)  16.1 us
    pad x18, local copies, waits for them, and re-layouts, local(): states = lax.associative_scan(combine, (decay, drive), axis=1)[1]  16 us
  transfers between devices with their start and end apart: 5, of which 4 were waited for; matrix products, arithmetic and copies ran while one was open for 27% of the time, Pallas kernels for 0%

commit v1 on v0

--- a/solution.py
+++ b/solution.py
@@ -8,11 +8,18 @@
 rate_scale = 8.0
 
 
+def gather_over(array, mesh_axis, d):
+    size = lax.axis_size(mesh_axis)
+    parts = jnp.stack([array for _ in range(size)])
+    parts = lax.all_to_all(parts, mesh_axis, split_axis=0, concat_axis=0)
+    return jnp.concatenate(parts, axis=d)
+
+
 def rows_first(arrays, axis, dims):
     turned = [jnp.moveaxis(a, dim, 0) for a, dim in zip(arrays, dims)]
     widths = [t[0].size for t in turned]
     both = jnp.concatenate([t.reshape(-1, w) for t, w in zip(turned, widths)], axis=1)
-    out = lax.all_gather(both, axis, axis=0, tiled=True)
+    out = gather_over(both, axis, 0)
     parts = jnp.split(out, [sum(widths[:k]) for k in range(1, len(widths))], axis=1)
     return tuple(
         (

time: 652 us -> 744 us (1.14)
  the two profiles are of different devices: /device:TPU:1 before, /device:TPU:35 now
where the time goes in v1:
time: 744 us; the launch traced here: 740 us
  waiting for transfers between devices  435 us (58%)
  local copies, waits for them, and re-layouts  136 us (18%)
  other arithmetic  60.8 us (8%)
  matrix products  45.8 us (6%)
  blocking collectives  41.2 us (6%)
  between operations  13.6 us (2%)
  starting transfers between devices  8.24 us (1%)
    all_to_all x1, waiting for transfers between devices, gather_over(): parts = lax.all_to_all(parts, mesh_axis, split_axis=0, concat_axis=0)  266 us
    all_gather x1, waiting for transfers between devices, side_by_side(): lax.all_gather(both, axis, axis=dim, tiled=True)  134 us
    slice x60, local copies, waits for them, and re-layouts, local(): states = lax.associative_scan(combine, (decay, drive), axis=1)[1]  107 us
    all_to_all x2, blocking collectives, summed_on_arrival(): lax.all_to_all(parts, axis, split_axis=0, concat_axis=0, tiled=True)  37.4 us
    dot_general x1, matrix products, local(): jnp.dot(activated, complete_contraction, preferred_element_type=jnp.float32)  25.6 us
    all_gather x1, waiting for transfers between devices, local(): stream_whole = lax.all_gather(stream_mid, 'tp', axis=1, tiled=True)  18.4 us
    mul x8, other arithmetic, combine(): return (earlier[0] * later[0], later[0] * earlier[1] + later[1])  15.9 us
  transfers between devices with their start and end apart: 5, of which 4 were waited for; matrix products, arithmetic and copies ran while one was open for 25% of the time, Pallas kernels for 0%

profile of v1, /device:TPU:35, one launch (start us, length us, event | category | flops | bytes accessed | tf_op | source)
XLA Modules:
  0.0 739.9 jit_solution(16734933471744537306)
XLA Ops:
  13.0 14.9 %all-gather.5.cloned.1.call-done = bf16[1,1024,2048]{2,1,0:T(8,128)(2,1)} async-done(((bf16[1,1024,1024]{2,1,0:T(8,128)(2,1)}), bf16[1,1024,2048]{2,1,0:T(8,128)(2,1)}) %all-gather.5.cloned.1.call-update) | async-done | bytes 4194320 | tf_op jit(solution)/shard_map/all_gather | solution.py:88
  31.0 133.9 %all-gather.7.cloned.1.call-done = bf16[2048,1024]{1,0:T(8,128)(2,1)} async-done(((bf16[64,1024]{1,0:T(8,128)(2,1)}), bf16[2048,1024]{1,0:T(8,128)(2,1)}) %all-gather.7.cloned.1.call-update) | async-done | bytes 4194320 | tf_op jit(solution)/shard_map/all_gather | solution.py:38
  164.9 5.2 fusion.39
  180.6 5.2 fusion.38
  185.8 6.3 slice.261
  192.2 6.2 slice.266
  198.4 6.2 slice.262
  204.6 3.6 slice.334
  215.2 3.7 fusion.83
  218.9 3.6 slice.272
  222.5 3.6 slice.268
  304.8 3.7 slice.267
  326.0 4.7 pad.84
  331.1 11.0 %convolution_convert_fusion = bf16[1024,2048]{1,0:T(8,128)(2,1)} fusion(bf16[512,2048]{0,1:T(8,128)(2,1)} %all-gather.9.cloned.1.call-done, f32[1,1024,512]{2,1,0:T(8,128)} %pad.84, f32[1,1024,512]{2,1,0:T(8,128)S(1)} %pad.85, bf16[2048,1024]{1,0:T(8,128)(2,1)} %all-gather.7.cloned.1.call-done, bf16[1,1024,2048]{2,1,0:T(8,128)(2,1)} %all-gather.5.cloned.1.call-done, ...), kind=kOutput, calls=%fused_computation.32 | convolution fusion | flops 4312268800 | bytes 16789504 | tf_op jit(solution)/shard_map/dot_general | solution.py:135
  344.7 29.2 %all_to_all.21 = bf16[2,1024,1024]{2,1,0:T(8,128)(2,1)} all-to-all(bf16[2,1024,1024]{2,1,0:T(8,128)(2,1)S(1)} %bitcast.69), channel_id=1, replica_groups=mesh['rep'=2,'fs'=32,'tp'=2] {'tp'}, dimensions={0} | all-to-all | bytes 8388608 | tf_op jit(solution)/shard_map/all_to_all | solution.py:48
  373.9 5.9 stack.2
  379.8 8.1 %all-to-all-start.1 = ((bf16[32,64,4096]{2,1,0:T(8,128)(2,1)}), bf16[32,64,4096]{2,1,0:T(8,128)(2,1)}, u32[]{:S(2)}, u32[]{:S(2)}) async-start(bf16[32,64,4096]{2,1,0:T(8,128)(2,1)} %stack.2), calls=%async_computation.1 | async-start | bytes 33554432 | tf_op jit(solution)/shard_map/all_to_all | solution.py:14
  388.0 4.0 convert_reduce_fusion.1
  396.3 18.4 %all-gather.11.cloned.1.call-done = bf16[1024,2048]{1,0:T(8,128)(2,1)} async-done(((bf16[1024,1024]{1,0:T(8,128)(2,1)}), bf16[1024,2048]{1,0:T(8,128)(2,1)}) %all-gather.11.cloned.1.call-update) | async-done | bytes 4194320 | tf_op jit(solution)/shard_map/all_gather | solution.py:147
  417.7 266.1 %all-to-all-done.1 = bf16[32,64,4096]{2,1,0:T(8,128)(2,1)} async-done(((bf16[32,64,4096]{2,1,0:T(8,128)(2,1)}), bf16[32,64,4096]{2,1,0:T(8,128)(2,1)}, u32[]{:S(2)}, u32[]{:S(2)}) %all-to-all-start.1) | async-done | bytes 16777248 | tf_op jit(solution)/shard_map/all_to_all | solution.py:14
  683.8 25.6 %fusion.21 = bf16[1024,2048]{1,0:T(8,128)(2,1)} fusion(bf16[2048,4096]{1,0:T(8,128)(2,1)} %bitcast.18, bf16[1024,2048]{1,0:T(8,128)(2,1)} %all-gather.11.cloned.1.call-done, f32[2048]{0:T(1024)S(1)} %copy-done.18, f32[1024]{0:T(1024)S(1)} %add_rsqrt_fusion.1), kind=kOutput, calls=%fused_computation.31 | convolution fusion | flops 17196646400 | bytes 25178112 | tf_op jit(solution)/shard_map/dot_general | solution.py:152
  712.1 8.2 %all_to_all.22 = bf16[2,1024,1024]{2,1,0:T(8,128)(2,1)S(1)} all-to-all(bf16[2,1024,1024]{2,1,0:T(8,128)(2,1)S(1)} %bitcast.70), channel_id=1, replica_groups=mesh['rep'=2,'fs'=32,'tp'=2] {'tp'}, dimensions={0} | all-to-all | bytes 8388608 | tf_op jit(solution)/shard_map/all_to_all | solution.py:48
  724.0 3.7 all_to_all.23
  727.8 5.6 fusion.18
  (176 shorter events, 139.4 us)
Async XLA Ops:
  6.5 166.3 %copy-start = (bf16[2,256,256]{2,1,0:T(8,128)(2,1)S(1)}, bf16[2,256,256]{2,1,0:T(8,128)(2,1)}, u32[]{:S(2)}) copy-start(bf16[2,256,256]{2,1,0:T(8,128)(2,1)} %param.20) | copy-start | bytes 786436
  6.5 158.4 %copy-start.16 = (f32[2048]{0:T(1024)S(1)}, f32[2048]{0:T(1024)}, u32[]{:S(2)}) copy-start(f32[2048]{0:T(1024)} %param.16) | copy-start | bytes 24580
  6.5 21.4 %all-gather.5.cloned.1.call-start = ((), (), s32[]{:S(2)}) async-start(), calls=%async_computation.4 | async-start | bytes 6291456 | tf_op jit(solution)/shard_map/all_gather | solution.py:88
  7.3 157.6 %all-gather.7.cloned.1.call-start = ((), (), s32[]{:S(2)}) async-start(), calls=%async_computation.5 | async-start | bytes 4325376 | tf_op jit(solution)/shard_map/all_gather | solution.py:38
  8.9 322.2 %all-gather.9.cloned.1.call-start = ((), (), s32[]{:S(2)}) async-start(), calls=%async_computation.6 | async-start | bytes 2162688 | tf_op jit(solution)/shard_map/all_gather | solution.py:137
  31.0 139.2 %copy-start.13 = (f32[1024]{0:T(1024)}, f32[1024]{0:T(1024)S(1)}, u32[]{:S(2)}) copy-start(f32[1024]{0:T(1024)S(1)} %add_rsqrt_fusion.2) | copy-start | bytes 12292
  174.9 1.8 copy-start.15
  178.7 1.9 copy-start.11
  308.5 9.5 %copy-start.9 = (f32[1,127,512]{2,1,0:T(8,128)S(1)}, f32[1,127,512]{2,1,0:T(8,128)}, u32[]{:S(2)}) copy-start(f32[1,127,512]{2,1,0:T(8,128)} %slice.273) | copy-start | bytes 780292
  308.5 9.5 %copy-start.10 = (f32[1,127,512]{2,1,0:T(8,128)S(1)}, f32[1,127,512]{2,1,0:T(8,128)}, u32[]{:S(2)}) copy-start(f32[1,127,512]{2,1,0:T(8,128)} %slice.330) | copy-start | bytes 780292
  318.5 5.7 copy-start.6
  325.9 4.9 copy-start.7
  325.9 5.2 copy-start.14
  325.9 5.2 copy-start.17
  344.7 29.2 %copy-start.8 = (bf16[64,4096]{1,0:T(8,128)(2,1)S(1)}, bf16[64,4096]{1,0:T(8,128)(2,1)}, u32[]{:S(2)}) copy-start(bf16[64,4096]{1,0:T(8,128)(2,1)} %pad_maximum_fusion.2) | copy-start | bytes 1572868
  379.8 304.0 %all-to-all-start.1 = ((bf16[32,64,4096]{2,1,0:T(8,128)(2,1)}), bf16[32,64,4096]{2,1,0:T(8,128)(2,1)}, u32[]{:S(2)}, u32[]{:S(2)}) async-start(bf16[32,64,4096]{2,1,0:T(8,128)(2,1)} %stack.2), calls=%async_computation.1 | async-start | bytes 33554432 | tf_op jit(solution)/shard_map/all_to_all | solution.py:14
  387.9 6.1 copy-start.4
  387.9 26.7 %all-gather.11.cloned.1.call-start = ((), (), s32[]{:S(2)}) async-start(), calls=%async_computation.7 | async-start | bytes 6291456 | tf_op jit(solution)/shard_map/all_gather | solution.py:147
  391.9 2.1 copy-start.2
  396.2 287.6 %copy-start.18 = (f32[2048]{0:T(1024)S(1)}, f32[2048]{0:T(1024)}, u32[]{:S(2)}) copy-start(f32[2048]{0:T(1024)} %param.24) | copy-start | bytes 24580
  720.3 3.0 copy-start.5
  721.4 2.0 copy-start.3
  723.3 4.4 copy-start.12
  727.7 5.6 copy-start.1
Sparse Core Ops, SparseCore 0:
  9.0 18.8 all-gather.4
  29.6 135.3 all-gather.6
  166.6 151.4 all-gather.8
  396.4 18.2 all-gather.10
